TPU v7x, 32 devices: a whole 2x2x4 slice. The times are simulated.
32 devices in a mesh: ep: 8 (over z, x), tp: 4 (over y, core).
Axes of the slice: x: 2, y: 2, z: 4, core: 2. Of those that a mesh axis runs over, the one named last changes fastest.
Arguments:
- glu_value: bfloat16 [32768, 1024], P(('ep', 'tp')), may hold values from -6 to 6
- glu_gate: bfloat16 [32768, 1024], P(('ep', 'tp')), may hold values from -6 to 6
- conv_taps: float32 [31, 1024], replicated, may hold values from -12 to 12
- chan_gain: float32 [1024], replicated, may hold values from 0.1 to 1.9
- chan_shift: float32 [1024], replicated, may hold values from -3 to 3
- mix_out_weight: bfloat16 [1024, 2048], P('tp'), may hold values from -0.1875 to 0.1875
- moe_input: bfloat16 [4096, 2048], P(('ep', 'tp')), may hold values from -6 to 6
- moe_gain: float32 [2048], replicated, may hold values from 0.1 to 1.9
- expert_ids: int32 [4096, 4], P(('ep', 'tp')), may hold values from 0 to 31, all different within a row; in each aligned block of 128 rows (0 to 127, 128 to 255, ...) at most 20 rows name the same one
- expert_share: float32 [4096, 4], P(('ep', 'tp')), may hold values from 0.05 to 1
- expert_gate_weight: bfloat16 [32, 2048, 1024], P(('ep', 'tp')), may hold values from -0.375 to 0.375
- expert_up_weight: bfloat16 [32, 2048, 1024], P(('ep', 'tp')), may hold values from -0.375 to 0.375
- expert_down_weight: bfloat16 [32, 1024, 2048], P(('ep', 'tp')), may hold values from -0.0390625 to 0.0390625
Outputs:
- mixed: bfloat16 [32768, 2048], P(('ep', 'tp'))
- moe_output: bfloat16 [4096, 2048], P(('ep', 'tp'))
Inputs may be any that keep to these rules, and one draw needn't show every extreme that they name: `expert_ids`: each row names 4 different experts. In each aligned block of 128 rows (the rows of one device) no expert is named by more than 20 rows, and in some block one expert is named by exactly 20 rows.
All inputs are finite; a program needn't handle non-finite values.
Results may differ from a plain program's by a relative error of at most 0.0071.
Values may be sent and summed in bfloat16 or wider, within the bound.
A program may use at most 192 MiB of HBM per device.

v0:
```python
import jax
import jax.numpy as jnp
from jax import lax
from jax.sharding import PartitionSpec as P

CLAMP_LIMIT = 7.0
GLU_SLOPE = 1.702


def passed_along(value, axis, steps):
    count = lax.axis_size(axis)
    first, last = (max(0, -steps), min(count, count - steps))
    return lax.ppermute(value, axis, [(source, source + steps) for source in range(first, last)])


def expert_apply(flat_rows, gate_matrix, up_matrix, down_matrix):
    pre_gate = jnp.dot(flat_rows, gate_matrix, preferred_element_type=jnp.float32)
    pre_up = jnp.dot(flat_rows, up_matrix, preferred_element_type=jnp.float32)
    gated = jnp.minimum(pre_gate, CLAMP_LIMIT)
    lifted = jnp.clip(pre_up, -CLAMP_LIMIT, CLAMP_LIMIT) + 1.0
    hidden = (lifted * gated * jax.nn.sigmoid(GLU_SLOPE * gated)).astype(jnp.bfloat16)
    return jnp.dot(hidden, down_matrix, preferred_element_type=jnp.float32).astype(jnp.bfloat16)


def body(
    glu_value,
    glu_gate,
    conv_taps,
    chan_gain,
    chan_shift,
    mix_out_weight,
    moe_input,
    moe_gain,
    expert_ids,
    expert_share,
    expert_gate_weight,
    expert_up_weight,
    expert_down_weight,
):
    positions = glu_value.shape[0]
    margin = conv_taps.shape[0] - 1
    borders = jnp.stack([glu_value[positions - margin :], glu_gate[positions - margin :]])
    earlier = passed_along(borders, ("ep", "tp"), 1)
    values_all = jnp.concatenate([earlier[0], glu_value], 0).astype(jnp.float32)
    gates_all = jnp.concatenate([earlier[1], glu_gate], 0).astype(jnp.float32)
    gated_input = values_all * jax.nn.sigmoid(gates_all)
    convolved = jnp.zeros(glu_value.shape, jnp.float32)
    for offset in range(margin + 1):
        convolved = convolved + conv_taps[offset] * gated_input[offset : offset + positions]
    center = jnp.mean(convolved, axis=-1, keepdims=True)
    spread = jnp.mean(jnp.square(convolved - center), axis=-1, keepdims=True)
    normalized = (convolved - center) * lax.rsqrt(spread + 1e-05) * chan_gain + chan_shift
    activated = jax.nn.silu(normalized).astype(jnp.bfloat16)
    mixed = jnp.dot(
        activated,
        lax.all_gather(mix_out_weight, "tp", axis=0, tiled=True),
        preferred_element_type=jnp.float32,
    ).astype(jnp.bfloat16)
    features = moe_input.astype(jnp.float32)
    scaled = features * lax.rsqrt(jnp.mean(jnp.square(features), axis=-1, keepdims=True) + 1e-06)
    moe_normed = (scaled * moe_gain).astype(jnp.bfloat16)
    tokens, per_token = expert_ids.shape
    model_width = moe_normed.shape[1]
    ep_size = lax.axis_size("ep")
    tp_size = lax.axis_size("tp")
    experts = ep_size * tp_size
    capacity = max(2, 5 * tokens * per_token // (4 * experts))
    copies = tokens * per_token
    flat_ids = expert_ids.reshape(copies)
    onehot = (flat_ids[:, None] == jnp.arange(experts, dtype=jnp.int32)[None, :]).astype(jnp.int32)
    earlier_count = jnp.sum((jnp.cumsum(onehot, axis=0) - onehot) * onehot, axis=1)
    slot_index = flat_ids * capacity + earlier_count
    slot_owner = (
        jnp.zeros((experts * capacity,), jnp.int32)
        .at[slot_index]
        .set(jnp.arange(copies, dtype=jnp.int32))
    )
    filled = jnp.zeros((experts * capacity,), jnp.bool_).at[slot_index].set(True)
    outgoing = jnp.where(
        filled[:, None], moe_normed[slot_owner // per_token], jnp.zeros((), jnp.bfloat16)
    )
    gate_matrix = expert_gate_weight[0]
    up_matrix = expert_up_weight[0]
    down_matrix = expert_down_weight[0]
    arrived = lax.all_to_all(
        outgoing.reshape(experts, capacity, model_width),
        ("ep", "tp"),
        split_axis=0,
        concat_axis=0,
        tiled=True,
    )
    sources = arrived.shape[0]
    held_slots = arrived.shape[1]
    answers = expert_apply(
        arrived.reshape(sources * held_slots, model_width), gate_matrix, up_matrix, down_matrix
    )
    answers = answers.reshape(sources, held_slots, model_width)
    returned = lax.all_to_all(answers, ("ep", "tp"), split_axis=0, concat_axis=0, tiled=True)
    picked = returned.reshape(experts * capacity, model_width)[slot_index].reshape(
        tokens, per_token, model_width
    )
    combined = jnp.zeros((tokens, model_width), jnp.float32)
    for choose in range(per_token):
        combined = combined + expert_share[:, choose : choose + 1] * picked[:, choose].astype(
            jnp.float32
        )
    return (mixed, combined.astype(jnp.bfloat16))


def solution(mesh):
    placed = (
        P(("ep", "tp"), None),
        P(("ep", "tp"), None),
        P(),
        P(),
        P(),
        P("tp", None),
        P(("ep", "tp"), None),
        P(),
        P(("ep", "tp"), None),
        P(("ep", "tp"), None),
        P(("ep", "tp"), None, None),
        P(("ep", "tp"), None, None),
        P(("ep", "tp"), None, None),
    )
    return jax.shard_map(
        body,
        mesh=mesh,
        in_specs=placed,
        out_specs=(P(("ep", "tp"), None), P(("ep", "tp"), None)),
        check_vma=False,
    )
```

profile of v0, /device:TPU:15, one launch (start us, length us, event | category | flops | bytes accessed | tf_op | source)
XLA Modules:
  0.0 242.7 jit_solution(7833906773496709997)
XLA Ops:
  7.2 0.7 broadcast_multiply_fusion.1
  7.8 0.8 copy.20
  8.6 0.1 eq.25
  8.7 0.1 eq.29
  8.9 1.2 fusion.46
  10.1 0.1 copy.19
  10.2 0.1 mul.523
  10.3 1.2 reduce-window.6
  11.5 0.2 slice_reduce_fusion
  11.8 0.1 fusion.57
  11.9 2.4 %scatter_custom_fusion.1 = s32[640]{0:T(1024)S(1)} fusion(s32[512]{0:T(512)S(1)} %bitcast.137, s32[512]{0:T(512)S(1)} %iota.11, s32[]{:T(128)} %constant.17.clone.1), kind=kCustom, calls=%fused_computation.126 | custom fusion | bytes 2564 | tf_op jit(solution)/shard_map/scatter | solution.py:76
  14.4 1.2 fusion.48
  15.6 4.1 %gather_fusion = bf16[640,2048]{1,0:T(8,128)(2,1)} fusion(bf16[128,2048]{1,0:T(8,128)(2,1)S(1)} %fusion.48, s32[1024]{0:T(1024)S(1)} %pad_clamp_fusion.1), kind=kCustom, calls=%fused_computation | custom fusion | bytes 5245440 | tf_op jit(solution)/shard_map/gather | solution.py:80
  19.7 3.5 %gather.9 = bf16[32,20,2048]{2,1,0:T(8,128)(2,1)S(1)} reshape(bf16[640,2048]{1,0:T(8,128)(2,1)} %gather_fusion) | data formatting | bytes 5242880 | tf_op jit(solution)/shard_map/gather | solution.py:80
  23.2 2.4 %scatter_custom_fusion = pred[640]{0:T(1024)(128)(4,1)S(1)} fusion(s32[512]{0:T(512)S(1)} %bitcast.138, pred[512]{0:T(512)(128)(4,1)S(1)} %broadcast.104, pred[]{:T(512)} %constant.25.clone.1), kind=kCustom, calls=%fused_computation.129 | custom fusion | bytes 641 | tf_op jit(solution)/shard_map/scatter | solution.py:78
  25.7 0.1 broadcast_in_dim.36
  25.8 2.0 broadcast_select_fusion
  27.8 6.2 %all-to-all-start = ((bf16[32,20,2048]{2,1,0:T(8,128)(2,1)}), bf16[32,20,2048]{2,1,0:T(8,128)(2,1)S(1)}, u32[]{:S(2)}, u32[]{:S(2)}) async-start(bf16[32,20,2048]{2,1,0:T(8,128)(2,1)} %broadcast_select_fusion), calls=%async_computation | async-start | bytes 6291456 | tf_op jit(solution)/shard_map/all_to_all | solution.py:85
  34.0 0.0 all-gather.2.cloned.1.call-start
  34.1 0.7 all-gather.2.cloned.1.call-update
  34.7 0.9 slice_bitcast_fusion.2
  35.7 3.6 %collective-permute-start = (bf16[2,30,1024]{2,1,0:T(8,128)(2,1)S(1)}, bf16[2,30,1024]{2,1,0:T(8,128)(2,1)S(1)}, u32[]{:S(2)}, u32[]{:S(2)}) collective-permute-start(bf16[2,30,1024]{2,1,0:T(8,128)(2,1)S(1)} %pad_maximum_fusion), channel_id=1, source_target_pairs={{0,1},{1,2},{2,3},{3,4},{4,5},{5,6},{6,7},{7,8},{8,9},{9,10},{10,1... | collective-permute-start | bytes 368648 | tf_op jit(solution)/shard_map/ppermute | solution.py:13
  39.2 0.0 copy-done.2
  39.3 0.1 fusion.73
  39.4 0.0 copy-done.3
  39.4 65.5 %collective-permute-done = bf16[2,30,1024]{2,1,0:T(8,128)(2,1)S(1)} collective-permute-done((bf16[2,30,1024]{2,1,0:T(8,128)(2,1)S(1)}, bf16[2,30,1024]{2,1,0:T(8,128)(2,1)S(1)}, u32[]{:S(2)}, u32[]{:S(2)}) %collective-permute-start) | collective-permute-done | bytes 122912 | tf_op jit(solution)/shard_map/ppermute | solution.py:13
  104.9 4.5 %divide_multiply_fusion = f32[1054,1024]{1,0:T(8,128)} fusion(bf16[1024,1024]{1,0:T(8,128)(2,1)} %param.13, bf16[30,1024]{1,0:T(8,128)(2,1)S(1)} %get-tuple-element.40, bf16[1024,1024]{1,0:T(8,128)(2,1)} %param.14, bf16[30,1024]{1,0:T(8,128)(2,1)S(1)} %get-tuple-element.39), kind=kLoop, calls=%fused_computation.4 | loop fusion | flops 12951552 | bytes 8634368 | tf_op jit(solution)/shard_map/mul | solution.py:46
  109.4 0.0 all-to-all-done
  109.4 2.2 reshape.102
  111.5 7.6 %fusion.34 = f32[640,1024]{1,0:T(8,128)} fusion(bf16[640,2048]{1,0:T(8,128)(2,1)} %reshape.102, bf16[1,2048,1024]{2,1,0:T(8,128)(2,1)} %param.24), kind=kOutput, calls=%fused_computation.70 | convolution fusion | flops 2684354560 | bytes 9437184 | tf_op jit(solution)/shard_map/dot_general | solution.py:18
  119.1 0.0 copy-done.1
  119.1 11.8 %fusion.36 = bf16[640,2048]{1,0:T(8,128)(2,1)} fusion(bf16[1,1024,2048]{2,1,0:T(8,128)(2,1)} %param.25, f32[640,1024]{1,0:T(8,128)} %fusion.34, bf16[640,2048]{1,0:T(8,128)(2,1)S(1)} %copy-done.1, bf16[1,2048,1024]{2,1,0:T(8,128)(2,1)} %param.23), kind=kOutput, calls=%fused_computation.75 | convolution fusion | flops 5376573440 | bytes 16252928 | tf_op jit(solution)/shard_map/dot_general | solution.py:22
  130.9 5.2 %reshape.103 = bf16[32,20,2048]{2,1,0:T(8,128)(2,1)} reshape(bf16[640,2048]{1,0:T(8,128)(2,1)} %fusion.36) | data formatting | bytes 5242880 | tf_op jit(solution)/shard_map/reshape | solution.py:97
  136.1 5.9 %all-to-all-start.1 = ((bf16[32,20,2048]{2,1,0:T(8,128)(2,1)}), bf16[32,20,2048]{2,1,0:T(8,128)(2,1)}, u32[]{:S(2)}, u32[]{:S(2)}) async-start(bf16[32,20,2048]{2,1,0:T(8,128)(2,1)} %reshape.103), calls=%async_computation.1 | async-start | bytes 6291456 | tf_op jit(solution)/shard_map/all_to_all | solution.py:98
  142.0 64.8 %fusion.70 = (f32[1024]{0:T(1024)S(1)}, f32[1024,1024]{1,0:T(8,128)S(1)}) fusion(f32[1054,1024]{1,0:T(8,128)} %divide_multiply_fusion, f32[1024]{0:T(1024)S(1)} %bitcast.116, f32[1024]{0:T(1024)S(1)} %bitcast.117, f32[1024]{0:T(1024)S(1)} %bitcast.119, f32[1024]{0:T(1024)S(1)} %bitcast.120, f32[1024]{0:T(1024)S(1)} %bitcast.121, f32[1024]{0:T(1024)S(1)} %bitcast.122, ...), kind=kLoop, calls=%fused_computation.142 | loop fusion | flops 65010688 | bytes 134348800 | tf_op jit(solution)/shard_map/reduce_sum | solution.py:50
  206.8 0.0 copy-start
  206.8 0.0 copy-start.4
  206.8 0.0 copy-start.5
  206.9 1.9 copy-done
  208.8 0.6 multiply_reduce_fusion
  209.3 0.0 all-gather.2.cloned.1.call-done
  209.4 10.7 %convolution_convert_fusion = bf16[1024,2048]{1,0:T(8,128)(2,1)} fusion(bf16[1024,2048]{1,0:T(8,128)(2,1)} %all-gather.2.cloned.1.call-done, f32[1024,1024]{1,0:T(8,128)} %copy-done, f32[1024]{0:T(1024)S(1)} %copy-done.4, f32[1024]{0:T(1024)S(1)} %copy-done.5, f32[1024]{0:T(1024)S(1)} %add_rsqrt_fusion, f32[1024]{0:T(1024)S(1)} %broadcast_multiply_fusion), kind=kOutput, calls=%fused_computation.74 | convolution fusion | flops 4306501632 | bytes 12599296 | tf_op jit(solution)/shard_map/dot_general | solution.py:54
  220.1 0.0 all-to-all-done.1
  220.1 3.6 %reshape.104 = bf16[640,2048]{1,0:T(8,128)(2,1)S(1)} reshape(bf16[32,20,2048]{2,1,0:T(8,128)(2,1)} %all-to-all-done.1) | data formatting | bytes 5242880 | tf_op jit(solution)/shard_map/reshape | solution.py:99
  223.7 3.3 %gather_fusion.1 = bf16[512,2048]{1,0:T(8,128)(2,1)} fusion(bf16[640,2048]{1,0:T(8,128)(2,1)S(1)} %reshape.104, s32[1024]{0:T(1024)S(1)} %pad_clamp_fusion), kind=kCustom, calls=%fused_computation.1 | custom fusion | bytes 4196352 | tf_op jit(solution)/shard_map/gather | solution.py:99
  227.1 2.7 %reshape.105 = bf16[128,4,2048]{2,1,0:T(4,128)(2,1)S(1)} reshape(bf16[512,2048]{1,0:T(8,128)(2,1)} %gather_fusion.1) | data formatting | bytes 4194304 | tf_op jit(solution)/shard_map/reshape | solution.py:99
  229.8 3.1 %fusion.72 = (bf16[128,1,2048]{2,1,0:T(2,128)(2,1)S(1)}, bf16[128,1,2048]{2,1,0:T(2,128)(2,1)S(1)}, bf16[128,1,2048]{2,1,0:T(2,128)(2,1)S(1)}, bf16[128,1,2048]{2,1,0:T(2,128)(2,1)S(1)}) fusion(bf16[128,4,2048]{2,1,0:T(4,128)(2,1)S(1)} %reshape.105), kind=kLoop, calls=%fused_computation.143 | loop fusion | bytes 4194304 | tf_op jit(solution)/shard_map/slice | solution.py:104
  232.9 3.0 %fusion.50 = bf16[128,2048]{1,0:T(8,128)(2,1)} fusion(bf16[128,1,2048]{2,1,0:T(2,128)(2,1)S(1)} %get-tuple-element.7, bf16[128,1,2048]{2,1,0:T(2,128)(2,1)S(1)} %get-tuple-element.5, bf16[128,1,2048]{2,1,0:T(2,128)(2,1)S(1)} %get-tuple-element.6, bf16[128,1,2048]{2,1,0:T(2,128)(2,1)S(1)} %get-tuple-element.4, f32[128]{0:T(128)S(1)} %get-tuple-element.43, ...), kind=kLoop, calls=%fused_computation.90 | loop fusion | flops 3145728 | bytes 2623488 | tf_op jit(solution)/shard_map/convert_element_type | solution.py:107
  (21 shorter events, 0.2 us)
Async XLA Ops:
  27.7 11.5 %copy-start.2 = (f32[31,1024]{1,0:T(8,128)S(1)}, f32[31,1024]{1,0:T(8,128)}, u32[]{:S(2)}) copy-start(f32[31,1024]{1,0:T(8,128)} %param.15) | copy-start | bytes 380932
  27.8 11.6 %copy-start.3 = (f32[128,4]{0,1:T(4,128)S(1)}, f32[128,4]{0,1:T(4,128)}, u32[]{:S(2)}) copy-start(f32[128,4]{0,1:T(4,128)} %param.22) | copy-start | bytes 6148
  27.8 81.6 %all-to-all-start = ((bf16[32,20,2048]{2,1,0:T(8,128)(2,1)}), bf16[32,20,2048]{2,1,0:T(8,128)(2,1)S(1)}, u32[]{:S(2)}, u32[]{:S(2)}) async-start(bf16[32,20,2048]{2,1,0:T(8,128)(2,1)} %broadcast_select_fusion), calls=%async_computation | async-start | bytes 6291456 | tf_op jit(solution)/shard_map/all_to_all | solution.py:85
  34.0 175.3 %all-gather.2.cloned.1.call-start = ((), (), s32[]{:S(2)}) async-start(), calls=%async_computation.2 | async-start | bytes 5242880 | tf_op jit(solution)/shard_map/all_gather | solution.py:56
  35.7 69.2 %collective-permute-start = (bf16[2,30,1024]{2,1,0:T(8,128)(2,1)S(1)}, bf16[2,30,1024]{2,1,0:T(8,128)(2,1)S(1)}, u32[]{:S(2)}, u32[]{:S(2)}) collective-permute-start(bf16[2,30,1024]{2,1,0:T(8,128)(2,1)S(1)} %pad_maximum_fusion), channel_id=1, source_target_pairs={{0,1},{1,2},{2,3},{3,4},{4,5},{5,6},{6,7},{7,8},{8,9},{9,10},{10,1... | collective-permute-start | bytes 368648 | tf_op jit(solution)/shard_map/ppermute | solution.py:13
  111.5 7.6 %copy-start.1 = (bf16[640,2048]{1,0:T(8,128)(2,1)S(1)}, bf16[640,2048]{1,0:T(8,128)(2,1)}, u32[]{:S(2)}) copy-start(bf16[640,2048]{1,0:T(8,128)(2,1)} %reshape.102) | copy-start | bytes 7864324
  136.1 84.0 %all-to-all-start.1 = ((bf16[32,20,2048]{2,1,0:T(8,128)(2,1)}), bf16[32,20,2048]{2,1,0:T(8,128)(2,1)}, u32[]{:S(2)}, u32[]{:S(2)}) async-start(bf16[32,20,2048]{2,1,0:T(8,128)(2,1)} %reshape.103), calls=%async_computation.1 | async-start | bytes 6291456 | tf_op jit(solution)/shard_map/all_to_all | solution.py:98
  206.8 1.9 copy-start
  206.8 2.5 %copy-start.4 = (f32[1024]{0:T(1024)S(1)}, f32[1024]{0:T(1024)}, u32[]{:S(2)}) copy-start(f32[1024]{0:T(1024)} %param.17) | copy-start | bytes 12292
  206.8 2.5 %copy-start.5 = (f32[1024]{0:T(1024)S(1)}, f32[1024]{0:T(1024)}, u32[]{:S(2)}) copy-start(f32[1024]{0:T(1024)} %param.16) | copy-start | bytes 12292
Sparse Core Ops, SparseCore 0:
  36.4 55.3 all-gather.1
where the time goes:
time: 245 us; the launch traced here: 243 us
  other arithmetic  79.3 us (32%)
  waiting for transfers between devices  66.2 us (27%)
  local copies, waits for them, and re-layouts  37.1 us (15%)
  matrix products  30.1 us (12%)
  starting transfers between devices  15.8 us (6%)
  between operations  14.3 us (6%)
    ppermute x1, waiting for transfers between devices, passed_along(): lax.ppermute(value, axis, [(source, source + steps) for source in range(f...  65.5 us
    reduce_sum x1, other arithmetic, body(): center = jnp.mean(convolved, axis=-1, keepdims=True)  64.8 us
    dot_general x1, matrix products, expert_apply(): jnp.dot(hidden, down_matrix, preferred_element_type=jnp.float32)  11.8 us
    dot_general x1, matrix products, body(): jnp.dot(activated, lax.all_gather(mix_out_weight, 'tp', axis=0, tiled=Tru...  10.7 us
    gather x2, local copies, waits for them, and re-layouts, body(): moe_normed[slot_owner // per_token]  7.58 us
    dot_general x1, matrix products, expert_apply(): pre_up = jnp.dot(flat_rows, up_matrix, preferred_element_type=jnp.float32)  7.57 us
    reshape x2, local copies, waits for them, and re-layouts, body(): returned.reshape(experts * capacity, model_width)[slot_index]  6.37 us
    all_to_all x1, starting transfers between devices, body(): lax.all_to_all(outgoing.reshape(experts, capacity, model_width), ('ep', '...  6.24 us
  transfers between devices with their start and end apart: 4, of which 1 were waited for; matrix products, arithmetic and copies ran while one was open for 45% of the time, Pallas kernels for 0%

commit v1 on v0

v1 whole, which is shorter than its diff:
```python
import functools

import jax
import jax.numpy as jnp
from jax import lax
from jax.experimental import pallas as pl
from jax.experimental.pallas import tpu as pltpu
from jax.sharding import PartitionSpec as P

CLAMP_LIMIT = 7.0
GLU_SLOPE = 1.702
LANES = 128
PACK = 16
MESH = pl.DeviceIdType.MESH
F32 = jnp.float32
BF16 = jnp.bfloat16


def place(flat, tp):
    return (flat // tp, flat % tp)


def greet(n, tp, me):
    barrier = pltpu.get_barrier_semaphore()

    @pl.loop(1, n)
    def _(k):
        pl.semaphore_signal(
            barrier, inc=1, device_id=place((me + k) % n, tp), device_id_type=MESH
        )

    pl.semaphore_wait(barrier, n - 1)


def slab(ref, index):
    return ref.at[pl.ds(pl.multiple_of(index * PACK, PACK), PACK)]


def exchange_copy(src, dst, ssem, rsem, me, n, tp, k):
    return pltpu.make_async_remote_copy(
        src_ref=slab(src, (me + k) % n),
        dst_ref=slab(dst, me),
        send_sem=ssem.at[k],
        recv_sem=rsem.at[k],
        device_id=place((me + k) % n, tp),
        device_id_type=MESH,
    )


def arrival(src, dst, ssem, rsem, me, n, tp, k):
    return pltpu.make_async_remote_copy(
        src_ref=slab(src, (me + k) % n),
        dst_ref=slab(dst, (me + n - k) % n),
        send_sem=ssem.at[k],
        recv_sem=rsem.at[k],
        device_id=place((me + k) % n, tp),
        device_id_type=MESH,
    )


def start_exchange(pairs, me, n, tp):
    @pl.loop(1, n)
    def _(k):
        for src, dst, ssem, rsem in pairs:
            exchange_copy(src, dst, ssem, rsem, me, n, tp, k).start()

    for src, dst, ssem, rsem in pairs:
        pltpu.make_async_copy(slab(src, me), slab(dst, me), ssem.at[0]).start()


def finish_exchange(pairs, me, n, tp):
    for src, dst, ssem, rsem in pairs:
        pltpu.make_async_copy(slab(src, me), slab(dst, me), ssem.at[0]).wait()

    @pl.loop(1, n)
    def _(k):
        for src, dst, ssem, rsem in pairs:
            copy = arrival(src, dst, ssem, rsem, me, n, tp, k)
            copy.wait_recv()
            copy.wait_send()


def first_kernel(
    n,
    tp,
    taps_count,
    margin,
    main,
    rest,
    value_all,
    gate_all,
    value,
    gate,
    taps,
    gain,
    shift,
    weight,
    main_out,
    rest_out,
    weight_out,
    act,
    halo_v,
    halo_g,
    glu,
    conv,
    main_s,
    main_r,
    rest_s,
    rest_r,
    halo_s,
    halo_r,
    weight_s,
    weight_r,
):
    step = pl.program_id(0)
    steps = pl.num_programs(0)
    e = lax.axis_index("ep")
    t = lax.axis_index("tp")
    me = e * tp + t
    rows, width = value.shape
    blocks = width // LANES
    depth = weight.shape[0]
    pairs = ((main, main_out, main_s, main_r), (rest, rest_out, rest_s, rest_r))
    positions = value_all.shape[0]

    def halo_copy(which, dest):
        src, dst = ((value_all, halo_v), (gate_all, halo_g))[which]
        return pltpu.make_async_remote_copy(
            src_ref=src.at[pl.ds(positions - margin, margin)],
            dst_ref=dst,
            send_sem=halo_s.at[which],
            recv_sem=halo_r.at[which],
            device_id=place(dest, tp),
            device_id_type=MESH,
        )

    def weight_copy(k, owner):
        return pltpu.make_async_remote_copy(
            src_ref=weight,
            dst_ref=weight_out.at[pl.ds(pl.multiple_of(owner * depth, depth), depth)],
            send_sem=weight_s.at[k],
            recv_sem=weight_r.at[k],
            device_id=(e, (t + k) % tp),
            device_id_type=MESH,
        )

    def own_weight():
        return pltpu.make_async_copy(
            weight,
            weight_out.at[pl.ds(pl.multiple_of(t * depth, depth), depth)],
            weight_s.at[0],
        )

    @pl.when(step == 0)
    def _():
        greet(n, tp, me)

        @pl.when(me < n - 1)
        def _():
            for which in range(2):
                halo_copy(which, me + 1).start()

        start_exchange(pairs, me, n, tp)
        for k in range(1, tp):
            weight_copy(k, t).start()
        own_weight().start()

        @pl.when(me > 0)
        def _():
            for which in range(2):
                halo_copy(which, me - 1).wait_recv()
            for b in range(blocks):
                cols = slice(b * LANES, (b + 1) * LANES)
                glu[b, 0:margin, :] = halo_v[:, cols].astype(F32) * jax.nn.sigmoid(
                    halo_g[:, cols].astype(F32)
                )

        @pl.when(me == 0)
        def _():
            for b in range(blocks):
                glu[b, 0:margin, :] = jnp.zeros((margin, LANES), F32)

    @pl.when(step > 0)
    def _():
        for b in range(blocks):
            glu[b, 0:margin, :] = glu[b, rows : rows + margin, :]

    for b in range(blocks):
        cols = slice(b * LANES, (b + 1) * LANES)
        glu[b, margin : margin + rows, :] = value[:, cols].astype(F32) * jax.nn.sigmoid(
            gate[:, cols].astype(F32)
        )

    part = 64
    lead = margin - (taps_count - 1)

    @pl.loop(0, rows // part)
    def _(r):
        base = r * part
        for b in range(blocks):
            cols = slice(b * LANES, (b + 1) * LANES)
            total = jnp.zeros((part, LANES), F32)
            for j in range(taps_count):
                total = total + taps[j : j + 1, cols] * glu[b, pl.ds(base + lead + j, part), :]
            conv[pl.ds(pl.multiple_of(base, part), part), cols] = total

    norm_part = 32

    @pl.loop(0, rows // norm_part)
    def _(r):
        rows_here = pl.ds(pl.multiple_of(r * norm_part, norm_part), norm_part)
        data = conv[rows_here, :]
        center = jnp.mean(data, axis=-1, keepdims=True)
        data = data - center
        spread = jnp.mean(data * data, axis=-1, keepdims=True)
        normed = data * lax.rsqrt(spread + 1e-05) * gain[...] + shift[...]
        act[rows_here, :] = (normed * jax.nn.sigmoid(normed)).astype(BF16)

    @pl.when(step == steps - 1)
    def _():
        @pl.when(me < n - 1)
        def _():
            for which in range(2):
                halo_copy(which, me + 1).wait_send()

        own_weight().wait()
        for k in range(1, tp):
            copy = weight_copy(k, (t + tp - k) % tp)
            copy.wait_recv()
            copy.wait_send()
        finish_exchange(pairs, me, n, tp)


def second_kernel(
    n, tp, main, rest, act, weight, main_out, rest_out, mixed, main_s, main_r, rest_s, rest_r
):
    step = pl.program_id(0)
    steps = pl.num_programs(0)
    me = lax.axis_index("ep") * tp + lax.axis_index("tp")
    pairs = ((main, main_out, main_s, main_r), (rest, rest_out, rest_s, rest_r))

    @pl.when(step == 0)
    def _():
        greet(n, tp, me)
        start_exchange(pairs, me, n, tp)

    mixed[...] = jnp.dot(act[...], weight[...], preferred_element_type=F32).astype(BF16)

    @pl.when(step == steps - 1)
    def _():
        finish_exchange(pairs, me, n, tp)


def fill(block):
    return pl.BlockSpec(block, lambda i: (0,) * len(block))


ANY = pl.BlockSpec(memory_space=pl.ANY)


def body(
    n,
    tp,
    glu_value,
    glu_gate,
    conv_taps,
    chan_gain,
    chan_shift,
    mix_out_weight,
    moe_input,
    moe_gain,
    expert_ids,
    expert_share,
    expert_gate_weight,
    expert_up_weight,
    expert_down_weight,
):
    tokens, per_token = expert_ids.shape
    copies = tokens * per_token
    width = moe_input.shape[1]
    capacity = max(2, 5 * copies // (4 * n))
    spare = 1
    while spare < capacity - PACK or (capacity < PACK and spare < capacity):
        spare *= 2
    has_main = capacity >= PACK
    base = PACK if has_main else 0
    cuts = PACK // spare
    piece = width // cuts
    slots = n * PACK

    features = moe_input.astype(F32)
    scaled = features * lax.rsqrt(jnp.mean(jnp.square(features), axis=-1, keepdims=True) + 1e-06)
    moe_normed = (scaled * moe_gain).astype(BF16)

    named = jnp.sum(
        (expert_ids[:, :, None] == jnp.arange(n, dtype=jnp.int32)).astype(BF16), axis=1
    )
    below = (
        jnp.arange(tokens)[:, None] > jnp.arange(tokens)[None, :]
    ).astype(BF16)
    before = jnp.dot(below, named, preferred_element_type=F32)
    hits = [
        (expert_ids[:, k : k + 1] == jnp.arange(n, dtype=jnp.int32)).astype(F32)
        for k in range(per_token)
    ]
    rank = [jnp.sum(before * hit, axis=1, keepdims=True).astype(jnp.int32) for hit in hits]
    main_code = [
        jnp.where(rank[k] < base, expert_ids[:, k : k + 1] * PACK + rank[k], -1)
        for k in range(per_token)
    ]
    rest_code = [
        jnp.where(rank[k] >= base, expert_ids[:, k : k + 1] * PACK + rank[k] - base, -slots)
        for k in range(per_token)
    ]
    lanes = jnp.arange(slots, dtype=jnp.int32)[None, :]

    def spread(codes, scales):
        total = jnp.zeros((tokens, slots), F32)
        for k in range(per_token):
            total = total + jnp.where(codes[k] == lanes, scales[k], 0.0)
        return total

    ones = [jnp.ones((tokens, 1), F32)] * per_token
    high = lax.reduce_precision(expert_share, 8, 7)
    low = expert_share - high
    highs = [high[:, k : k + 1] for k in range(per_token)]
    lows = [low[:, k : k + 1] for k in range(per_token)]

    def pick(matrix, data):
        return lax.dot_general(
            matrix, data, (((0,), (0,)), ((), ())), preferred_element_type=F32
        ).astype(BF16)

    def pieces(data):
        return jnp.concatenate([data[:, q * piece : (q + 1) * piece] for q in range(cuts)], axis=0)

    def rest_place(scales):
        return [
            spread([code + q * spare for code in rest_code], scales).astype(BF16)
            for q in range(cuts)
        ]

    if has_main:
        main = pick(spread(main_code, ones).astype(BF16), moe_normed)
    else:
        main = jnp.zeros((slots, LANES), BF16)
    rest = pick(jnp.concatenate(rest_place(ones), axis=0), pieces(moe_normed))

    positions, channels = glu_value.shape
    taps_count = conv_taps.shape[0]
    margin = -(-(taps_count - 1) // PACK) * PACK
    tile = min(256, positions)
    steps = positions // tile
    dma = pltpu.SemaphoreType.DMA
    row_tile = pl.BlockSpec((tile, channels), lambda i: (i, 0))
    out_width = mix_out_weight.shape[1]
    main_in, rest_in, weight, act = pl.pallas_call(
        functools.partial(first_kernel, n, tp, taps_count, margin),
        grid=(steps,),
        name="dispatch_and_conv",
        out_shape=(
            jax.ShapeDtypeStruct(main.shape, BF16),
            jax.ShapeDtypeStruct(rest.shape, BF16),
            jax.ShapeDtypeStruct((channels, out_width), BF16),
            jax.ShapeDtypeStruct((positions, channels), BF16),
        ),
        in_specs=[
            ANY,
            ANY,
            ANY,
            ANY,
            row_tile,
            row_tile,
            fill(conv_taps.shape),
            fill((1, channels)),
            fill((1, channels)),
            pl.BlockSpec(memory_space=pltpu.VMEM),
        ],
        out_specs=(ANY, ANY, ANY, row_tile),
        scratch_shapes=[
            pltpu.VMEM((margin, channels), BF16),
            pltpu.VMEM((margin, channels), BF16),
            pltpu.VMEM((channels // LANES, margin + tile, LANES), F32),
            pltpu.VMEM((tile, channels), F32),
            dma((n,)),
            dma((n,)),
            dma((n,)),
            dma((n,)),
            dma((2,)),
            dma((2,)),
            dma((tp,)),
            dma((tp,)),
        ],
        compiler_params=pltpu.CompilerParams(
            collective_id=0,
            has_side_effects=True,
            dimension_semantics=("arbitrary",),
            vmem_limit_bytes=32 * 1024 * 1024,
        ),
    )(
        main,
        rest,
        glu_value,
        glu_gate,
        glu_value,
        glu_gate,
        conv_taps,
        chan_gain.reshape(1, channels),
        chan_shift.reshape(1, channels),
        mix_out_weight,
    )

    row = jnp.arange(n * spare, dtype=jnp.int32)
    home = (row // spare) * PACK + row % spare
    selectors = [
        ((home + q * spare)[:, None] == jnp.arange(slots, dtype=jnp.int32)[None, :]).astype(BF16)
        for q in range(cuts)
    ]
    opened = jnp.concatenate(
        [jnp.dot(s, rest_in, preferred_element_type=F32).astype(BF16) for s in selectors], axis=1
    )
    flat_rows = jnp.concatenate([main_in, opened], axis=0) if has_main else opened
    pre_gate = jnp.dot(flat_rows, expert_gate_weight[0], preferred_element_type=F32)
    pre_up = jnp.dot(flat_rows, expert_up_weight[0], preferred_element_type=F32)
    gated = jnp.minimum(pre_gate, CLAMP_LIMIT)
    lifted = jnp.clip(pre_up, -CLAMP_LIMIT, CLAMP_LIMIT) + 1.0
    hidden = (lifted * gated * jax.nn.sigmoid(GLU_SLOPE * gated)).astype(BF16)
    answers = jnp.dot(hidden, expert_down_weight[0], preferred_element_type=F32).astype(BF16)
    if has_main:
        main_answers, rest_answers = answers[:slots], answers[slots:]
    else:
        main_answers, rest_answers = main_in, answers
    rest_answers = pick(jnp.concatenate(selectors, axis=0), pieces(rest_answers))

    main_back, rest_back, mixed = pl.pallas_call(
        functools.partial(second_kernel, n, tp),
        grid=(steps,),
        name="return_and_mix",
        out_shape=(
            jax.ShapeDtypeStruct(main.shape, BF16),
            jax.ShapeDtypeStruct(rest.shape, BF16),
            jax.ShapeDtypeStruct((positions, out_width), BF16),
        ),
        in_specs=[ANY, ANY, row_tile, fill((channels, out_width))],
        out_specs=(ANY, ANY, pl.BlockSpec((tile, out_width), lambda i: (i, 0))),
        scratch_shapes=[dma((n,)), dma((n,)), dma((n,)), dma((n,))],
        compiler_params=pltpu.CompilerParams(
            collective_id=1,
            has_side_effects=True,
            dimension_semantics=("arbitrary",),
            vmem_limit_bytes=32 * 1024 * 1024,
        ),
    )(main_answers, rest_answers, act, weight)

    def weigh(parts, data):
        both = jnp.dot(jnp.concatenate(parts, axis=0), data, preferred_element_type=F32)
        return both[:tokens] + both[tokens:]

    highs_rest, lows_rest = rest_place(highs), rest_place(lows)
    combined = jnp.concatenate(
        [weigh([highs_rest[q], lows_rest[q]], rest_back) for q in range(cuts)], axis=1
    )
    if has_main:
        combined = combined + weigh(
            [spread(main_code, highs).astype(BF16), spread(main_code, lows).astype(BF16)],
            main_back,
        )
    return (mixed, combined.astype(BF16))


def solution(mesh):
    tp = mesh.shape["tp"]
    n = mesh.shape["ep"] * tp
    both = P(("ep", "tp"), None)
    weights = P(("ep", "tp"), None, None)
    placed = (
        both, both, P(), P(), P(), P("tp", None), both, P(), both, both, weights, weights, weights
    )
    return jax.shard_map(
        functools.partial(body, n, tp),
        mesh=mesh,
        in_specs=placed,
        out_specs=(both, both),
        check_vma=False,
    )
```

time: 245 us -> 200 us (0.82)
  Pallas kernels: 0 us -> 152 us
  other arithmetic: 79.3 us -> 8.62 us
  waiting for transfers between devices: 66.2 us -> 0 us
  local copies, waits for them, and re-layouts: 37.1 us -> 10.4 us
  starting transfers between devices: 15.8 us -> 0 us
  between operations: 14.3 us -> 1.26 us
  matrix products: 30.1 us -> 27.3 us
    pallas_call x0 -> x2, Pallas kernels: none -> 152 us  [the longest x1 81.7 us: body(): pl.pallas_call(functools.partial(first_kernel, n, tp, taps_count, margin)...]
    ppermute x1 -> x0, waiting for transfers between devices: 65.5 us -> none  [passed_along(): lax.ppermute(value, axis, [(source, source + steps) for source in range(f...]
    reduce_sum x3 -> x1, other arithmetic: 65.4 us -> 0.69 us  [body(): jnp.sum((expert_ids[:, :, None] == jnp.arange(n, dtype=jnp.int32)).astype...]
    reshape x4 -> x0, local copies, waits for them, and re-layouts: 13.7 us -> none  [the longest x2 6.37 us: body(): returned.reshape(experts * capacity, model_width)[slot_index]]
    all_to_all x2 -> x0, starting transfers between devices: 12.2 us -> none  [the longest x1 6.24 us: body(): lax.all_to_all(outgoing.reshape(experts, capacity, model_width), ('ep', '...]
    gather x3 -> x0, local copies, waits for them, and re-layouts: 10.9 us -> none  [the longest x2 7.58 us: body(): moe_normed[slot_owner // per_token]]
    unnamed x13 -> x67, local copies, waits for them, and re-layouts: 2.69 us -> 8.08 us
    mul x2 -> x0, other arithmetic: 5.18 us -> none  [the longest x1 4.49 us: body(): gated_input = values_all * jax.nn.sigmoid(gates_all)]
  transfers between devices with their start and end apart: 4 -> 0, of which waited for: 1 -> 0; matrix products, arithmetic and copies ran while one was open for 45% -> 0% of each run, Pallas kernels for 0% -> 0%
where the time goes in v1:
time: 200 us
  Pallas kernels  152 us (76%)
  matrix products  27.3 us (14%)
  local copies, waits for them, and re-layouts  10.4 us (5%)
  other arithmetic  8.62 us (4%)
    pallas_call x1, Pallas kernels, body(): pl.pallas_call(functools.partial(first_kernel, n, tp, taps_count, margin)...  81.7 us
    pallas_call x1, Pallas kernels, body(): pl.pallas_call(functools.partial(second_kernel, n, tp), grid=(steps,), na...  70.5 us
    dot_general x1, matrix products, body(): jnp.dot(hidden, expert_down_weight[0], preferred_element_type=F32)  17.9 us
    unnamed x67, local copies, waits for them, and re-layouts  8.08 us
    dot_general x1, matrix products, body(): pre_up = jnp.dot(flat_rows, expert_up_weight[0], preferred_element_type=F32)  4.45 us

profile of v1, /device:TPU:15, one launch (start us, length us, event | category | flops | bytes accessed | tf_op | source)
XLA Modules:
  0.0 199.8 jit_solution(606264831864495363)
XLA Ops:
  0.6 0.0 copy-start.10
  0.6 0.8 slice_bitcast_fusion.10
  1.5 0.7 fusion.74
  2.2 0.2 select_reduce_fusion.3
  2.3 0.8 add_bitcast_fusion.11
  3.3 0.7 fusion.97
  4.0 0.6 add_convert_fusion.5
  4.6 0.6 add_convert_fusion.9
  5.2 1.2 fusion.11
  6.4 0.9 fusion.13
  7.4 0.0 copy-start
  7.4 0.0 copy-start.1
  7.4 0.0 copy-start.4
  7.4 0.0 copy-start.5
  7.4 0.0 copy-start.6
  7.5 0.0 copy-start.7
  7.5 0.5 convolution_convert_fusion.2.rest
  8.0 0.9 convolution_convert_fusion.main
  8.9 0.1 copy-done
  9.0 0.6 copy-done.1
  9.6 0.3 copy-done.4
  9.9 81.7 %dispatch_and_conv.1 = (bf16[512,2048]{1,0:T(8,128)(2,1)S(1)}, bf16[512,512]{1,0:T(8,128)(2,1)S(1)}, bf16[1024,2048]{1,0:T(8,128)(2,1)S(1)}, bf16[1024,1024]{1,0:T(8,128)(2,1)S(1)}) custom-call(bf16[512,2048]{1,0:T(8,128)(2,1)S(1)} %convolution_convert_fusion.main, bf16[512,512]{1,0:T(8,128)(2,1)S(1)} %convolution_convert_fusion.2.rest, ...), custom_call_target="tpu_custom_call" | custom-call | tf_op jit(solution)/shard_map/dispatch_and_conv/pallas_call | solution.py:357
  91.6 2.0 %copy-done.2 = bf16[1024,2048]{1,0:T(8,128)(2,1)} copy-done((bf16[1024,2048]{1,0:T(8,128)(2,1)}, bf16[1024,2048]{1,0:T(8,128)(2,1)S(1)}, u32[]{:S(2)}) %copy-start.2) | copy-done | bytes 4194328
  93.6 0.3 convolution_convert_fusion.3
  93.9 0.2 copy-done.30
  94.2 0.3 convolution_convert_fusion.4
  94.5 0.3 convolution_convert_fusion.5
  94.8 0.3 convolution_convert_fusion.6
  95.1 0.2 copy-done.29
  95.3 0.4 copy-done.11
  95.7 4.4 %fusion.4 = f32[640,1024]{1,0:T(8,128)} fusion(bf16[1,2048,1024]{2,1,0:T(8,128)(2,1)S(1)} %copy-done.32, bf16[128,512]{1,0:T(8,128)(2,1)S(1)} %convolution_convert_fusion.3, bf16[128,512]{1,0:T(8,128)(2,1)S(1)} %convolution_convert_fusion.4, bf16[128,512]{1,0:T(8,128)(2,1)S(1)} %convolution_convert_fusion.5, ...), kind=kOutput, calls=%fused_computation.4 | convolution fusion | flops 2697461760 | bytes 9437184 | tf_op jit(solution)/shard_map/dot_general | solution.py:424
  100.2 17.9 %fusion.6 = bf16[640,2048]{1,0:T(8,128)(2,1)} fusion(bf16[1,1024,2048]{2,1,0:T(8,128)(2,1)} %param.25, f32[640,1024]{1,0:T(8,128)} %fusion.4, bf16[1,2048,1024]{2,1,0:T(8,128)(2,1)} %param.23, bf16[128,512]{1,0:T(8,128)(2,1)S(1)} %convolution_convert_fusion.3, bf16[128,512]{1,0:T(8,128)(2,1)S(1)} %convolution_convert_fusion.4, ...), kind=kOutput, calls=%fused_computation.6 | convolution fusion | flops 5389680640 | bytes 16252928 | tf_op jit(solution)/shard_map/dot_general | solution.py:428
  118.1 1.3 fusion.95
  119.4 0.8 iota_compare_fusion
  120.2 0.8 iota_compare_fusion.2
  121.0 0.5 convolution_convert_fusion.1.rest
  121.5 0.0 copy-start.3
  121.5 0.1 slice.141.main
  121.7 2.0 %copy-done.3 = bf16[1024,2048]{1,0:T(8,128)(2,1)S(1)} copy-done((bf16[1024,2048]{1,0:T(8,128)(2,1)S(1)}, bf16[1024,2048]{1,0:T(8,128)(2,1)}, u32[]{:S(2)}) %copy-start.3) | copy-done | bytes 4194328
  123.7 70.5 %return_and_mix.1 = (bf16[512,2048]{1,0:T(8,128)(2,1)S(1)}, bf16[512,512]{1,0:T(8,128)(2,1)S(1)}, bf16[1024,2048]{1,0:T(8,128)(2,1)S(1)}) custom-call(bf16[512,2048]{1,0:T(8,128)(2,1)S(1)} %slice.141.main, bf16[512,512]{1,0:T(8,128)(2,1)S(1)} %convolution_convert_fusion.1.rest, bf16[1024,1024]{1,0:T(8,128)(2,1)S(1)} %get-tuple-element.11.act, ...), custom_call_target="tpu_custom_call" | custom-call | tf_op jit(solution)/shard_map/return_and_mix/pallas_call | solution.py:435
  194.2 0.3 fusion.58
  194.6 0.3 fusion.54
  195.0 0.3 fusion.50
  195.4 0.3 fusion.46
  195.8 0.3 add_convert_fusion.1
  196.1 0.7 fusion.62
  196.8 1.0 fusion.15
  197.8 2.0 %copy.25 = bf16[1024,2048]{1,0:T(8,128)(2,1)} copy(bf16[1024,2048]{1,0:T(8,128)(2,1)S(1)} %get-tuple-element.99) | data formatting | bytes 8388608
  (63 shorter events, 0.3 us)
Async XLA Ops:
  0.6 5.8 %copy-start.10 = (bf16[128,2048]{1,0:T(8,128)(2,1)S(1)}, bf16[128,2048]{1,0:T(8,128)(2,1)}, u32[]{:S(2)}) copy-start(bf16[128,2048]{1,0:T(8,128)(2,1)} %param.19) | copy-start | bytes 1572868
  3.2 4.7 %copy-start.20 = (s32[128]{0:T(128)}, s32[128]{0:T(128)S(1)}, u32[]{:S(2)}) copy-start(s32[128]{0:T(128)S(1)} %get-tuple-element.36) | copy-start | bytes 1540
  3.2 4.7 %copy-start.22 = (s32[128]{0:T(128)}, s32[128]{0:T(128)S(1)}, u32[]{:S(2)}) copy-start(s32[128]{0:T(128)S(1)} %get-tuple-element.64) | copy-start | bytes 1540
  3.2 4.7 %copy-start.24 = (s32[128]{0:T(128)}, s32[128]{0:T(128)S(1)}, u32[]{:S(2)}) copy-start(s32[128]{0:T(128)S(1)} %get-tuple-element.67) | copy-start | bytes 1540
  3.2 4.7 %copy-start.26 = (s32[128]{0:T(128)}, s32[128]{0:T(128)S(1)}, u32[]{:S(2)}) copy-start(s32[128]{0:T(128)S(1)} %get-tuple-element.70) | copy-start | bytes 1540
  4.0 3.4 %copy-start.12 = (f32[128]{0:T(128)}, f32[128]{0:T(128)S(1)}, u32[]{:S(2)}) copy-start(f32[128]{0:T(128)S(1)} %get-tuple-element.89) | copy-start | bytes 1540
  4.0 3.4 %copy-start.14 = (f32[128]{0:T(128)}, f32[128]{0:T(128)S(1)}, u32[]{:S(2)}) copy-start(f32[128]{0:T(128)S(1)} %get-tuple-element.90) | copy-start | bytes 1540
  4.0 3.4 %copy-start.16 = (f32[128]{0:T(128)}, f32[128]{0:T(128)S(1)}, u32[]{:S(2)}) copy-start(f32[128]{0:T(128)S(1)} %get-tuple-element.91) | copy-start | bytes 1540
  4.0 3.4 %copy-start.18 = (f32[128]{0:T(128)}, f32[128]{0:T(128)S(1)}, u32[]{:S(2)}) copy-start(f32[128]{0:T(128)S(1)} %get-tuple-element.92) | copy-start | bytes 1540
  7.4 1.6 copy-start
  7.4 2.2 %copy-start.1 = (bf16[1024,1024]{1,0:T(8,128)(2,1)S(1)}, bf16[1024,1024]{1,0:T(8,128)(2,1)}, u32[]{:S(2)}) copy-start(bf16[1024,1024]{1,0:T(8,128)(2,1)} %gate.1) | copy-start | bytes 6291460
  7.4 2.5 %copy-start.4 = (bf16[256,2048]{1,0:T(8,128)(2,1)S(1)}, bf16[256,2048]{1,0:T(8,128)(2,1)}, u32[]{:S(2)}) copy-start(bf16[256,2048]{1,0:T(8,128)(2,1)} %weight.1) | copy-start | bytes 3145732
  7.4 2.5 %copy-start.5 = (f32[31,1024]{1,0:T(8,128)S(1)}, f32[31,1024]{1,0:T(8,128)}, u32[]{:S(2)}) copy-start(f32[31,1024]{1,0:T(8,128)} %taps.1) | copy-start | bytes 380932
  7.4 2.4 %copy-start.6 = (f32[1024]{0:T(1024)S(1)}, f32[1024]{0:T(1024)}, u32[]{:S(2)}) copy-start(f32[1024]{0:T(1024)} %param.16) | copy-start | bytes 12292
  7.5 2.4 %copy-start.7 = (f32[1024]{0:T(1024)S(1)}, f32[1024]{0:T(1024)}, u32[]{:S(2)}) copy-start(f32[1024]{0:T(1024)} %param.17) | copy-start | bytes 12292
  9.9 85.8 %copy-start.32 = (bf16[1,2048,1024]{2,1,0:T(8,128)(2,1)S(1)}, bf16[1,2048,1024]{2,1,0:T(8,128)(2,1)}, u32[]{:S(2)}) copy-start(bf16[1,2048,1024]{2,1,0:T(8,128)(2,1)} %param.24) | copy-start | bytes 12582916
  91.6 2.0 %copy-start.2 = (bf16[1024,2048]{1,0:T(8,128)(2,1)}, bf16[1024,2048]{1,0:T(8,128)(2,1)S(1)}, u32[]{:S(2)}) copy-start(bf16[1024,2048]{1,0:T(8,128)(2,1)S(1)} %get-tuple-element.12.weight) | copy-start | bytes 12582916
  93.6 1.4 copy-start.8
  93.6 0.5 copy-start.30
  94.2 0.9 copy-start.31
  94.4 0.6 copy-start.28
  94.7 0.6 copy-start.29
  95.0 0.7 copy-start.11
  118.1 3.4 %copy-start.9 = (bf16[640,2048]{1,0:T(8,128)(2,1)S(1)}, bf16[640,2048]{1,0:T(8,128)(2,1)}, u32[]{:S(2)}) copy-start(bf16[640,2048]{1,0:T(8,128)(2,1)} %fusion.6) | copy-start | bytes 7864324
  121.5 2.2 %copy-start.3 = (bf16[1024,2048]{1,0:T(8,128)(2,1)S(1)}, bf16[1024,2048]{1,0:T(8,128)(2,1)}, u32[]{:S(2)}) copy-start(bf16[1024,2048]{1,0:T(8,128)(2,1)} %copy-done.2) | copy-start | bytes 12582916
  194.9 0.8 copy-start.13
  194.9 0.8 copy-start.15
  194.9 0.8 copy-start.17
  194.9 0.8 copy-start.19
  194.9 0.8 copy-start.21
  194.9 0.8 copy-start.23
  195.0 0.8 copy-start.25
  195.0 0.8 copy-start.27

commit v2 on v1

--- a/solution.py
+++ b/solution.py
@@ -59,8 +59,9 @@
 
 
 def start_exchange(pairs, me, n, tp):
-    @pl.loop(1, n)
-    def _(k):
+    @pl.loop(0, n - 1)
+    def _(j):
+        k = 1 + (j + n // 4 - 1) % (n - 1)
         for src, dst, ssem, rsem in pairs:
             exchange_copy(src, dst, ssem, rsem, me, n, tp, k).start()
 
@@ -134,15 +135,30 @@
             device_id_type=MESH,
         )
 
-    def weight_copy(k, owner):
+    sibling = t + 1 - 2 * (t % 2)
+
+    def weight_rows(owner):
+        return weight_out.at[pl.ds(pl.multiple_of(owner * depth, depth), depth)]
+
+    def weight_copy(src, owner, dest, k):
         return pltpu.make_async_remote_copy(
-            src_ref=weight,
-            dst_ref=weight_out.at[pl.ds(pl.multiple_of(owner * depth, depth), depth)],
+            src_ref=src,
+            dst_ref=weight_rows(owner),
             send_sem=weight_s.at[k],
             recv_sem=weight_r.at[k],
-            device_id=(e, (t + k) % tp),
+            device_id=(e, dest),
             device_id_type=MESH,
         )
+
+    def weight_far(k, owner):
+        return weight_copy(weight, owner, (t + k) % tp, k)
+
+    def weight_relay(k):
+        owner = (t + tp - k) % tp
+        return weight_copy(weight_rows(owner), owner, sibling, k + 1)
+
+    def weight_relayed(k):
+        return weight_copy(weight, (sibling + tp - k) % tp, sibling, k + 1)
 
     def own_weight():
         return pltpu.make_async_copy(
@@ -160,9 +176,10 @@
             for which in range(2):
                 halo_copy(which, me + 1).start()
 
+        for k in range(2, tp, 2):
+            weight_far(k, t).start()
+        weight_copy(weight, t, sibling, 1).start()
         start_exchange(pairs, me, n, tp)
-        for k in range(1, tp):
-            weight_copy(k, t).start()
         own_weight().start()
 
         @pl.when(me > 0)
@@ -191,6 +208,12 @@
             gate[:, cols].astype(F32)
         )
 
+    @pl.when(step == steps - 1)
+    def _():
+        for k in range(2, tp, 2):
+            weight_far(k, (t + tp - k) % tp).wait_recv()
+            weight_relay(k).start()
+
     part = 64
     lead = margin - (taps_count - 1)
 
@@ -224,11 +247,70 @@
                 halo_copy(which, me + 1).wait_send()
 
         own_weight().wait()
-        for k in range(1, tp):
-            copy = weight_copy(k, (t + tp - k) % tp)
-            copy.wait_recv()
-            copy.wait_send()
+        weight_copy(weight, sibling, sibling, 1).wait_recv()
+        weight_copy(weight, t, sibling, 1).wait_send()
+        for k in range(2, tp, 2):
+            weight_far(k, t).wait_send()
+            weight_relayed(k).wait_recv()
+            weight_relay(k).wait_send()
         finish_exchange(pairs, me, n, tp)
+
+
+def expert_kernel(
+    has_main, n, spare, cuts, main, rest, gate, up, down, main_out, rest_out, rows, total
+):
+    step = pl.program_id(0)
+    slots = n * PACK
+    count = n * spare
+    piece = main_out.shape[1] // cuts if has_main else total.shape[1] // cuts
+    first = slots if has_main else 0
+    bits = spare.bit_length() - 1
+
+    def home(shape, dim, q):
+        row = lax.broadcasted_iota(jnp.int32, shape, dim)
+        slot = lax.broadcasted_iota(jnp.int32, shape, 1 - dim)
+        where = (row >> bits) * PACK + (row & (spare - 1)) + q * spare
+        return (where == slot).astype(F32).astype(BF16)
+
+    @pl.when(step == 0)
+    def _():
+        if has_main:
+            rows[0:slots, :] = main[...]
+        for q in range(cuts):
+            rows[first : first + count, q * piece : (q + 1) * piece] = jnp.dot(
+                home((count, slots), 0, q), rest[...], preferred_element_type=F32
+            ).astype(BF16)
+
+    data = rows[...]
+    pre_gate = jnp.dot(data, gate[0], preferred_element_type=F32)
+    pre_up = jnp.dot(data, up[0], preferred_element_type=F32)
+    gated = jnp.minimum(pre_gate, CLAMP_LIMIT)
+    lifted = jnp.clip(pre_up, -CLAMP_LIMIT, CLAMP_LIMIT) + 1.0
+    hidden = (lifted * gated * jax.nn.sigmoid(GLU_SLOPE * gated)).astype(BF16)
+    part = jnp.dot(hidden, down[0], preferred_element_type=F32)
+
+    @pl.when(step == 0)
+    def _():
+        total[...] = part
+
+    @pl.when(step > 0)
+    def _():
+        total[...] += part
+
+    @pl.when(step == pl.num_programs(0) - 1)
+    def _():
+        if has_main:
+            main_out[...] = total[0:slots, :].astype(BF16)
+        else:
+            main_out[...] = main[...]
+        folded = jnp.zeros(rest.shape, F32)
+        for q in range(cuts):
+            folded = folded + jnp.dot(
+                home((slots, count), 1, q),
+                total[first : first + count, q * piece : (q + 1) * piece].astype(BF16),
+                preferred_element_type=F32,
+            )
+        rest_out[...] = folded.astype(BF16)
 
 
 def second_kernel(
@@ -410,27 +492,31 @@
         mix_out_weight,
     )
 
-    row = jnp.arange(n * spare, dtype=jnp.int32)
-    home = (row // spare) * PACK + row % spare
-    selectors = [
-        ((home + q * spare)[:, None] == jnp.arange(slots, dtype=jnp.int32)[None, :]).astype(BF16)
-        for q in range(cuts)
-    ]
-    opened = jnp.concatenate(
-        [jnp.dot(s, rest_in, preferred_element_type=F32).astype(BF16) for s in selectors], axis=1
-    )
-    flat_rows = jnp.concatenate([main_in, opened], axis=0) if has_main else opened
-    pre_gate = jnp.dot(flat_rows, expert_gate_weight[0], preferred_element_type=F32)
-    pre_up = jnp.dot(flat_rows, expert_up_weight[0], preferred_element_type=F32)
-    gated = jnp.minimum(pre_gate, CLAMP_LIMIT)
-    lifted = jnp.clip(pre_up, -CLAMP_LIMIT, CLAMP_LIMIT) + 1.0
-    hidden = (lifted * gated * jax.nn.sigmoid(GLU_SLOPE * gated)).astype(BF16)
-    answers = jnp.dot(hidden, expert_down_weight[0], preferred_element_type=F32).astype(BF16)
-    if has_main:
-        main_answers, rest_answers = answers[:slots], answers[slots:]
-    else:
-        main_answers, rest_answers = main_in, answers
-    rest_answers = pick(jnp.concatenate(selectors, axis=0), pieces(rest_answers))
+    hidden_units = expert_gate_weight.shape[2]
+    block = min(256, hidden_units)
+    count = (slots if has_main else 0) + n * spare
+    columns = pl.BlockSpec((1, width, block), lambda f: (0, 0, f))
+    main_answers, rest_answers = pl.pallas_call(
+        functools.partial(expert_kernel, has_main, n, spare, cuts),
+        grid=(hidden_units // block,),
+        name="experts",
+        out_shape=(
+            jax.ShapeDtypeStruct(main.shape, BF16),
+            jax.ShapeDtypeStruct(rest.shape, BF16),
+        ),
+        in_specs=[
+            fill(main.shape),
+            fill(rest.shape),
+            columns,
+            columns,
+            pl.BlockSpec((1, block, width), lambda f: (0, f, 0)),
+        ],
+        out_specs=(fill(main.shape), fill(rest.shape)),
+        scratch_shapes=[pltpu.VMEM((count, width), BF16), pltpu.VMEM((count, width), F32)],
+        compiler_params=pltpu.CompilerParams(
+            dimension_semantics=("arbitrary",), vmem_limit_bytes=44 * 1024 * 1024
+        ),
+    )(main_in, rest_in, expert_gate_weight, expert_up_weight, expert_down_weight)
 
     main_back, rest_back, mixed = pl.pallas_call(
         functools.partial(second_kernel, n, tp),

time: 200 us -> 161 us (0.81)
  matrix products: 27.3 us -> 3.39 us
  local copies, waits for them, and re-layouts: 10.4 us -> 4.18 us
  Pallas kernels: 152 us -> 147 us
  other arithmetic: 8.62 us -> 5.2 us
    dot_general x6 -> x0, matrix products: 23.4 us -> none  [the longest x1 17.9 us: body(): jnp.dot(hidden, expert_down_weight[0], preferred_element_type=F32)]
    pallas_call x0 -> x1, Pallas kernels: none -> 14.2 us  [body(): pl.pallas_call(functools.partial(expert_kernel, has_main, n, spare, cuts)...]
    pallas_call x1, Pallas kernels: 81.7 us -> 68 us  [body(): pl.pallas_call(functools.partial(first_kernel, n, tp, taps_count, margin)...]
    pallas_call x1, Pallas kernels: 70.5 us -> 64.8 us  [body(): pl.pallas_call(functools.partial(second_kernel, n, tp), grid=(steps,), na...]
    unnamed x67 -> x19, local copies, waits for them, and re-layouts: 8.08 us -> 3.3 us
where the time goes in v2:
time: 161 us
  Pallas kernels  147 us (91%)
  other arithmetic  5.2 us (3%)
  local copies, waits for them, and re-layouts  4.18 us (3%)
  matrix products  3.39 us (2%)
    pallas_call x1, Pallas kernels, body(): pl.pallas_call(functools.partial(first_kernel, n, tp, taps_count, margin)...  68 us
    pallas_call x1, Pallas kernels, body(): pl.pallas_call(functools.partial(second_kernel, n, tp), grid=(steps,), na...  64.8 us
    pallas_call x1, Pallas kernels, body(): pl.pallas_call(functools.partial(expert_kernel, has_main, n, spare, cuts)...  14.2 us
    unnamed x19, local copies, waits for them, and re-layouts  3.3 us

profile of v2, /device:TPU:15, one launch (start us, length us, event | category | flops | bytes accessed | tf_op | source)
XLA Modules:
  0.0 160.7 jit_solution(11303066304859223852)
XLA Ops:
  0.6 0.0 copy-start.7
  0.6 0.0 copy-start.8
  0.6 0.8 slice_bitcast_fusion.10
  1.5 0.7 fusion.47
  2.2 0.2 select_reduce_fusion.3
  2.4 0.8 add_bitcast_fusion.11
  3.2 0.7 fusion.61
  3.9 0.6 add_convert_fusion.5
  4.5 0.6 add_convert_fusion.9
  5.1 0.0 copy-done.7
  5.1 0.2 fusion
  5.3 0.0 copy-done.8
  5.3 0.2 fusion.2
  5.6 0.0 copy-start.1
  5.6 0.0 copy-start.3
  5.6 0.5 convolution_convert_fusion.1.rest
  6.1 0.0 copy-start
  6.1 0.0 copy-start.4
  6.1 0.0 copy-start.5
  6.1 0.0 copy-start.6
  6.1 0.9 convolution_convert_fusion.main
  7.0 0.2 copy-done.1
  7.2 0.3 copy-done.3
  7.4 0.8 copy-done
  8.2 0.0 copy-done.4
  8.2 0.0 copy-done.5
  8.2 0.0 copy-done.6
  8.2 0.0 copy-start.2
  8.2 68.0 %dispatch_and_conv.1 = (bf16[512,2048]{1,0:T(8,128)(2,1)S(1)}, bf16[512,512]{1,0:T(8,128)(2,1)S(1)}, bf16[1024,2048]{1,0:T(8,128)(2,1)S(1)}, bf16[1024,1024]{1,0:T(8,128)(2,1)S(1)}) custom-call(bf16[512,2048]{1,0:T(8,128)(2,1)S(1)} %convolution_convert_fusion.main, bf16[512,512]{1,0:T(8,128)(2,1)S(1)} %convolution_convert_fusion.1.rest, ...), custom_call_target="tpu_custom_call" | custom-call | tf_op jit(solution)/shard_map/dispatch_and_conv/pallas_call | solution.py:439
  76.3 0.0 copy-done.2
  76.3 14.2 %experts.1 = (bf16[512,2048]{1,0:T(8,128)(2,1)S(1)}, bf16[512,512]{1,0:T(8,128)(2,1)S(1)}) custom-call(bf16[512,2048]{1,0:T(8,128)(2,1)S(1)} %get-tuple-element.11.main, bf16[512,512]{1,0:T(8,128)(2,1)S(1)} %get-tuple-element.12.rest, bf16[1,2048,1024]{2,1,0:T(8,128)(2,1)S(1)} %copy-done.2, bf16[1,2048,1024]{2,1,0:T(8,128)(2,1)} %up.1, ...), custom_call_target="tpu_custom_call" | custom-call | tf_op jit(solution)/shard_map/experts/pallas_call | solution.py:499
  90.5 64.8 %return_and_mix.1 = (bf16[512,2048]{1,0:T(8,128)(2,1)S(1)}, bf16[512,512]{1,0:T(8,128)(2,1)S(1)}, bf16[1024,2048]{1,0:T(8,128)(2,1)S(1)}) custom-call(bf16[512,2048]{1,0:T(8,128)(2,1)S(1)} %get-tuple-element.13.main, bf16[512,512]{1,0:T(8,128)(2,1)S(1)} %get-tuple-element.14.rest, bf16[1024,1024]{1,0:T(8,128)(2,1)S(1)} %get-tuple-element.15.act, ...), custom_call_target="tpu_custom_call" | custom-call | tf_op jit(solution)/shard_map/return_and_mix/pallas_call | solution.py:521
  155.3 0.3 fusion.31
  155.7 0.3 fusion.27
  156.0 0.3 fusion.23
  156.4 0.3 fusion.19
  156.7 0.3 add_convert_fusion.1
  157.0 0.7 fusion.35
  157.7 1.0 fusion.4
  158.7 2.0 %copy.17 = bf16[1024,2048]{1,0:T(8,128)(2,1)} copy(bf16[1024,2048]{1,0:T(8,128)(2,1)S(1)} %get-tuple-element.95) | data formatting | bytes 8388608
  (9 shorter events, 0.2 us)
Async XLA Ops:
  0.6 4.5 %copy-start.7 = (bf16[128,2048]{1,0:T(8,128)(2,1)S(1)}, bf16[128,2048]{1,0:T(8,128)(2,1)}, u32[]{:S(2)}) copy-start(bf16[128,2048]{1,0:T(8,128)(2,1)} %param.19) | copy-start | bytes 1572868
  0.6 4.7 %copy-start.8 = (f32[2048]{0:T(1024)S(1)}, f32[2048]{0:T(1024)}, u32[]{:S(2)}) copy-start(f32[2048]{0:T(1024)} %param.20) | copy-start | bytes 24580
  5.6 1.6 copy-start.1
  5.6 1.8 %copy-start.3 = (bf16[256,2048]{1,0:T(8,128)(2,1)S(1)}, bf16[256,2048]{1,0:T(8,128)(2,1)}, u32[]{:S(2)}) copy-start(bf16[256,2048]{1,0:T(8,128)(2,1)} %weight.1) | copy-start | bytes 3145732
  6.1 2.2 %copy-start = (bf16[1024,1024]{1,0:T(8,128)(2,1)S(1)}, bf16[1024,1024]{1,0:T(8,128)(2,1)}, u32[]{:S(2)}) copy-start(bf16[1024,1024]{1,0:T(8,128)(2,1)} %value.1) | copy-start | bytes 6291460
  6.1 2.2 %copy-start.4 = (f32[31,1024]{1,0:T(8,128)S(1)}, f32[31,1024]{1,0:T(8,128)}, u32[]{:S(2)}) copy-start(f32[31,1024]{1,0:T(8,128)} %taps.1) | copy-start | bytes 380932
  6.1 2.2 %copy-start.5 = (f32[1024]{0:T(1024)S(1)}, f32[1024]{0:T(1024)}, u32[]{:S(2)}) copy-start(f32[1024]{0:T(1024)} %param.16) | copy-start | bytes 12292
  6.1 2.1 %copy-start.6 = (f32[1024]{0:T(1024)S(1)}, f32[1024]{0:T(1024)}, u32[]{:S(2)}) copy-start(f32[1024]{0:T(1024)} %param.17) | copy-start | bytes 12292
  8.2 68.0 %copy-start.2 = (bf16[1,2048,1024]{2,1,0:T(8,128)(2,1)S(1)}, bf16[1,2048,1024]{2,1,0:T(8,128)(2,1)}, u32[]{:S(2)}) copy-start(bf16[1,2048,1024]{2,1,0:T(8,128)(2,1)} %gate.3) | copy-start | bytes 12582916
